TPU v7x, 32 devices: a whole 2x2x4 slice. The times are simulated.
32 devices in a mesh: grp: 2 (over y), kv: 4 (over z), tp: 4 (over x, core).
Axes of the slice: x: 2, y: 2, z: 4, core: 2. Of those that a mesh axis runs over, the one named last changes fastest.
Arguments:
- tokens: bfloat16 [24, 4096], P('grp', 'kv'), parts along dimension 0, may hold values from -25 to 25
- mix_gain: bfloat16 [4096], P('kv'), may hold values from 0.099609375 to 1.8984375
- query_weight: bfloat16 [4096, 2048], P('kv', 'tp'), may hold values from -0.09375 to 0.09375
- key_weight: bfloat16 [4096, 2048], P('kv', 'tp'), may hold values from -0.09375 to 0.09375
- decay_weight: bfloat16 [4096, 2048], P('kv', 'tp'), may hold values from -0.09375 to 0.09375
- value_weight: bfloat16 [4096, 4096], P('kv', 'tp'), may hold values from -0.09375 to 0.09375
- gate_weight: bfloat16 [4096, 4096], P('kv', 'tp'), may hold values from -0.09375 to 0.09375
- state: float32 [24, 8, 256, 512], P(('grp', 'kv'), 'tp'), parts along dimension 0, may hold values from -6 to 6
- block_keys: bfloat16 [24, 64, 2048], P(('grp', 'kv'), None, 'tp'), parts along dimension 0, may hold values from -6 to 6
- block_values: bfloat16 [24, 64, 4096], P(('grp', 'kv'), None, 'tp'), parts along dimension 0, may hold values from -6 to 6
- block_decay: float32 [24, 64, 2048], P(('grp', 'kv'), None, 'tp'), parts along dimension 0, as said below
- lengths: int32 [24], P(('grp', 'kv')), parts along dimension 0, may hold values from 1 to 64, 384 in all
- head_gain: bfloat16 [512], replicated, may hold values from 0.099609375 to 1.8984375
- out_weight: bfloat16 [4096, 4096], P('tp', 'kv'), may hold values from -0.09375 to 0.09375
- mlp_gain: bfloat16 [4096], P('kv'), may hold values from 0.099609375 to 1.8984375
- up_weight: bfloat16 [4096, 16384], P('kv', 'tp'), may hold values from -0.09375 to 0.09375
- down_weight: bfloat16 [16384, 4096], P('tp', 'kv'), may hold values from -0.046875 to 0.046875
Outputs:
- result: bfloat16 [24, 4096], P('grp', 'kv'), parts along dimension 0
There are 2 independent parts, one for each index of `grp`. A program takes and returns all parts, laid end to end along the dimension named above; an argument that names none is the same for every part. Nothing has to cross between parts.
Inputs may be any that keep to these rules, and one draw needn't show every extreme that they name: `block_decay`: along a row's block positions the values never rise. In each part the 12 lengths add up to 384, and the largest is 64.
All inputs are finite; a program needn't handle non-finite values. No bound on the sum of `lengths` on one device may be relied on, other than what follows from the above.
Results may differ from a plain program's by a relative error of at most 0.0062.
Values may be sent and summed in bfloat16 or wider, within the bound.
A program may use at most 64 MiB of HBM per device.

v0:
```python
import functools

import jax
import jax.numpy as jnp
from jax import lax
from jax.experimental import pallas as pl
from jax.experimental.pallas import tpu as pltpu
from jax.sharding import PartitionSpec as P

EPSILON = 1e-06
MESH = pl.DeviceIdType.MESH
F32, BF16 = jnp.float32, jnp.bfloat16
ANY = pl.BlockSpec(memory_space=pl.ANY)


def kernel(
    cfg,
    tokens, mix_gain, wq, wk, wd, wv, wg, state, keys, values, decay, lengths,
    head_gain, wo, mlp_gain, wu, wdn,
    out,
    tok_v, mix_v, wq_v, wk_v, wd_v, wv_v, wg_v, state_v, keys_v, values_v, decay_v,
    hg_v, wo_v, mg_v, wu_v, wdn_v,
    slab_a, slab_b, recv_a, recv_b, gath, outx, sq_own, sq_recv, mlp_lhs,
    up_send, up_recv, sq_mine, sq_all, acc, downx,
    state_b, kw_v,
    load_sem, a_s, a_r, b_s, b_r, g_s, g_r, o_s, o_r, q_s, q_r, u_s, u_r, c_s, c_r, d_s, d_r,
):
    n_kv, n_tp, width, S, SP, PR, rs = cfg
    rows = tok_v.shape[0]
    hk = state_v.shape[2]
    hv = state_v.shape[3]
    heads = state_v.shape[1]
    positions = keys_v.shape[1]
    kcols = wq_v.shape[1]
    vcols = wv_v.shape[1]
    me = lax.axis_index("kv")
    mt = lax.axis_index("tp")

    def kv_peer(d):
        return lax.rem(me + d, n_kv)

    def tp_peer(d):
        return lax.rem(mt + d, n_tp)

    loads = {}
    pairs = [
        (tokens, tok_v), (mix_gain, mix_v), (wq, wq_v), (wk, wk_v), (wd, wd_v), (wv, wv_v), (wg, wg_v),
        (decay, decay_v), (keys, keys_v), (state, state_v), (values, values_v),
        (head_gain, hg_v), (wo, wo_v), (mlp_gain, mg_v), (wu, wu_v), (wdn, wdn_v),
    ]
    for at, (src, dst) in enumerate(pairs):
        copy = pltpu.make_async_copy(src, dst, load_sem.at[at])
        copy.start()
        loads[id(dst)] = copy

    def ready(ref):
        loads[id(ref)].wait()

    barrier = pltpu.get_barrier_semaphore()
    for d in range(1, n_kv):
        pl.semaphore_signal(barrier, inc=1, device_id={"kv": kv_peer(d)}, device_id_type=MESH)
    for d in range(1, n_tp):
        pl.semaphore_signal(barrier, inc=1, device_id={"tp": tp_peer(d)}, device_id_type=MESH)

    def to_kv(src, dst, send, recv, d):
        return pltpu.make_async_remote_copy(
            src_ref=src, dst_ref=dst, send_sem=send.at[d], recv_sem=recv.at[d],
            device_id={"kv": kv_peer(d)}, device_id_type=MESH)

    def to_tp(src, dst, send, recv, d):
        return pltpu.make_async_remote_copy(
            src_ref=src, dst_ref=dst, send_sem=send.at[d], recv_sem=recv.at[d],
            device_id={"tp": tp_peer(d)}, device_id_type=MESH)

    ready(tok_v)
    ready(mix_v)
    tok = tok_v[...].astype(F32)
    scaled = tok * mix_v[...].astype(F32)[None, :]
    squares = jnp.sum(tok * tok, axis=1, keepdims=True)
    if PR > rows:
        scaled = jnp.concatenate([scaled, jnp.zeros((PR - rows, scaled.shape[1]), F32)], axis=0)
        squares = jnp.concatenate([squares, jnp.zeros((PR - rows, 1), F32)], axis=0)
    scaled = scaled.astype(BF16)
    squares = jnp.broadcast_to(squares, (PR, 128))
    high = squares.astype(BF16).astype(F32)
    low = squares - high

    def spread(part, slab, at):
        for k in range(n_kv):
            slab[k, :, at:at + part.shape[1]] = part[k * S:k * S + SP].astype(BF16)

    spread(high, slab_a, 3 * kcols)
    spread(low, slab_a, 3 * kcols + 128)
    for at, ref in enumerate((wq_v, wk_v, wd_v)):
        ready(ref)
        spread(jnp.dot(scaled, ref[...], preferred_element_type=F32), slab_a, at * kcols)
    pl.semaphore_wait(barrier, n_kv + n_tp - 2)
    a_copies = [to_kv(slab_a.at[kv_peer(d)], recv_a.at[d], a_s, a_r, d) for d in range(1, n_kv)]
    for copy in a_copies:
        copy.start()
    for at, ref in enumerate((wv_v, wg_v)):
        ready(ref)
        spread(jnp.dot(scaled, ref[...], preferred_element_type=F32), slab_b, at * vcols)
    b_copies = [to_kv(slab_b.at[kv_peer(d)], recv_b.at[d], b_s, b_r, d) for d in range(1, n_kv)]
    for copy in b_copies:
        copy.start()

    ready(decay_v)
    ready(keys_v)
    position = lax.broadcasted_iota(jnp.int32, (positions, kcols), 0)
    befores = []
    for b in range(S):
        length = lengths[b]
        log = decay_v[b]
        before = jnp.sum(jnp.where(position == length - 1, log, 0.0), axis=0, keepdims=True)
        befores.append(before)
        rel = jnp.where(position < length, before - log, -jnp.inf)
        kw_v[b] = (jnp.exp(rel) * keys_v[b].astype(F32)).astype(BF16)
    if SP > S:
        befores.append(jnp.zeros((SP - S, kcols), F32))
    before = jnp.concatenate(befores, axis=0)
    ready(state_v)
    for b in range(S):
        for h in range(heads):
            state_b[b, h] = state_v[b, h].astype(BF16)
    ready(values_v)
    ready(hg_v)

    for copy in a_copies:
        copy.wait_recv()
    got = slab_a[me].astype(F32)
    for d in range(1, n_kv):
        got = got + recv_a[d].astype(F32)
    total = got[:, 3 * kcols:3 * kcols + 1] + got[:, 3 * kcols + 128:3 * kcols + 129]
    inverse = lax.rsqrt(total / width + EPSILON)
    query = got[:, :kcols] * inverse * hk ** (-0.5)
    key = got[:, kcols:2 * kcols] * inverse
    x = got[:, 2 * kcols:3 * kcols] * inverse
    log_decay = (jnp.minimum(x, 0.0) - jnp.log1p(jnp.exp(-jnp.abs(x)))) / 16.0
    carry_query = (query * jnp.exp(before + log_decay)).astype(BF16)
    block_query = (query * jnp.exp(log_decay)).astype(BF16)
    product = query * key
    heads_out = []
    for h in range(heads):
        cols = slice(h * hk, (h + 1) * hk)
        attended = []
        for b in range(S):
            scores = lax.dot_general(
                block_query[:, cols], kw_v[b, :, h * hk:(h + 1) * hk],
                (((1,), (1,)), ((), ())), preferred_element_type=F32)
            both = jnp.dot(carry_query[:, cols], state_b[b, h], preferred_element_type=F32)
            both = both + jnp.dot(
                scores.astype(BF16), values_v[b, :, h * hv:(h + 1) * hv],
                preferred_element_type=F32)
            attended.append(both[b:b + 1])
        if SP > S:
            attended.append(jnp.zeros((SP - S, hv), F32))
        heads_out.append(jnp.concatenate(attended, axis=0))

    for copy in b_copies:
        copy.wait_recv()
    got = slab_b[me].astype(F32)
    for d in range(1, n_kv):
        got = got + recv_b[d].astype(F32)
    gain = hg_v[...].astype(F32)[None, :]
    for h in range(heads):
        value = got[:, h * hv:(h + 1) * hv] * inverse
        gate = got[:, vcols + h * hv:vcols + (h + 1) * hv] * inverse
        own = jnp.sum(product[:, h * hk:(h + 1) * hk], axis=1, keepdims=True)
        att = heads_out[h] + own * value
        norm = att * lax.rsqrt(jnp.mean(att * att, axis=1, keepdims=True) + EPSILON)
        gath[me, :, h * hv:(h + 1) * hv] = (norm * gain * (gate * jax.nn.sigmoid(gate))).astype(BF16)
    g_copies = [to_kv(gath.at[me], gath.at[me], g_s, g_r, d) for d in range(1, n_kv)]
    for copy in g_copies:
        copy.start()

    ready(wo_v)
    for copy in g_copies:
        copy.wait_recv()
    merged = jnp.concatenate([gath[k].astype(F32)[:S] for k in range(n_kv)], axis=0).astype(BF16)
    outx[mt] = jnp.dot(merged, wo_v[...], preferred_element_type=F32).astype(BF16)
    o_copies = [to_tp(outx.at[mt], outx.at[mt], o_s, o_r, d) for d in range(1, n_tp)]
    for copy in o_copies:
        copy.start()
    ready(mg_v)
    for copy in o_copies:
        copy.wait_recv()
    summed = outx[0].astype(F32)
    for t in range(1, n_tp):
        summed = summed + outx[t].astype(F32)
    mixed = (tok_v[...].astype(F32) + summed).astype(BF16).astype(F32)

    sq_own[...] = jnp.broadcast_to(jnp.sum(mixed * mixed, axis=1, keepdims=True), (rows, 128))
    q_copies = [to_kv(sq_own, sq_recv.at[d], q_s, q_r, d) for d in range(1, n_kv)]
    for copy in q_copies:
        copy.start()
    mlp_lhs[...] = (mixed * mg_v[...].astype(F32)[None, :]).astype(BF16)
    ready(wu_v)
    rr, cw = up_send.shape[1:]

    def place(p):
        return pl.multiple_of((p // rs) * cw, 128), lax.rem(p, rs) * rr

    def up_of(p):
        col, row = place(p)
        left = mlp_lhs[...] if rs == 1 else mlp_lhs[pl.ds(pl.multiple_of(row, 16), rr), :]
        return jnp.dot(left, wu_v[:, pl.ds(col, cw)], preferred_element_type=F32)

    def up_step(d, carry):
        up_send[d] = up_of(kv_peer(d)).astype(BF16)
        to_kv(up_send.at[d], up_recv.at[d], u_s, u_r, d).start()
        return carry

    far_first = sorted(range(1, n_kv), key=lambda d: -min(d, n_kv - d))
    if n_kv <= 8:
        for d in far_first:
            up_step(d, 0)
    else:
        lax.fori_loop(1, n_kv, up_step, 0)
    pre = up_of(me)
    for copy in q_copies:
        copy.wait_recv()
    sq_total = sq_own[...]
    for d in range(1, n_kv):
        sq_total = sq_total + sq_recv[d]
    sq_mine[...] = lax.rsqrt(sq_total / width + EPSILON)
    if rs == 1:
        inverse_mlp = sq_mine[...]
    else:
        inverse_mlp = sq_mine[pl.ds(pl.multiple_of(place(me)[1], 8), rr), :]
    for d in range(1, n_kv):
        to_kv(up_send.at[d], up_recv.at[d], u_s, u_r, d).wait_recv()
        pre = pre + up_recv[d].astype(F32)
    act = jnp.maximum(pre * inverse_mlp[:, :1], 0.0)
    sq_all[0] = (act * act).astype(BF16)
    c_copies = [to_kv(sq_all.at[0], sq_all.at[d], c_s, c_r, d) for d in range(1, n_kv)]
    for copy in c_copies:
        copy.start()
    ready(wdn_v)
    if rs > 1:
        acc[...] = jnp.zeros_like(acc)

    def down_of(d):
        col, row = place(lax.rem(me - d + n_kv, n_kv))
        part = jnp.dot(sq_all[d], wdn_v[pl.ds(col, cw), :], preferred_element_type=F32)
        return part, row

    def add_down(d):
        part, row = down_of(d)
        if rs == 1:
            acc[...] += part
        else:
            at = pl.ds(pl.multiple_of(row, 8), rr)
            acc[at, :] = acc[at, :] + part

    if rs == 1:
        acc[...] = down_of(0)[0]
    else:
        add_down(0)

    def down_step(d, carry):
        to_kv(sq_all.at[0], sq_all.at[d], c_s, c_r, d).wait_recv()
        add_down(d)
        return carry

    if n_kv <= 8:
        for d in far_first[::-1]:
            down_step(d, 0)
    else:
        lax.fori_loop(1, n_kv, down_step, 0)
    downx[mt] = acc[...].astype(BF16)
    d_copies = [to_tp(downx.at[mt], downx.at[mt], d_s, d_r, d) for d in range(1, n_tp)]
    for copy in d_copies:
        copy.start()
    for copies in (a_copies, b_copies, g_copies, o_copies, q_copies, c_copies):
        for copy in copies:
            copy.wait_send()
    for d in range(1, n_kv):
        to_kv(up_send.at[d], up_recv.at[d], u_s, u_r, d).wait_send()
    for copy in d_copies:
        copy.wait_recv()
    summed = downx[0].astype(F32)
    for t in range(1, n_tp):
        summed = summed + downx[t].astype(F32)
    out[...] = (mixed + summed).astype(BF16)
    for copy in d_copies:
        copy.wait_send()


def on_device(n_kv, n_tp, *args):
    tokens, wq, wv, state, keys, wu, wdn = (args[i] for i in (0, 2, 5, 7, 8, 15, 16))
    rows, depth = tokens.shape
    S = state.shape[0]
    SP = (S + 3) // 4 * 4
    PR = ((n_kv - 1) * S + SP + 15) // 16 * 16
    kcols, vcols, hidden = wq.shape[1], wv.shape[1], wu.shape[1]
    col_splits = min(n_kv, hidden // 128)
    rs = n_kv // col_splits
    rr, cw = rows // rs, hidden // col_splits
    loaded = [args[i] for i in (0, 1, 2, 3, 4, 5, 6, 7, 8, 9, 10, 12, 13, 14, 15, 16)]
    V = pltpu.VMEM
    dma_kv = pltpu.SemaphoreType.DMA((n_kv,))
    dma_tp = pltpu.SemaphoreType.DMA((n_tp,))
    wa, wb = 3 * kcols + 256, 2 * vcols
    scratch = [V(a.shape, a.dtype) for a in loaded] + [
        V((n_kv, SP, wa), BF16), V((n_kv, SP, wb), BF16),
        V((n_kv, SP, wa), BF16), V((n_kv, SP, wb), BF16),
        V((n_kv, SP, vcols), BF16), V((n_tp, rows, depth), BF16),
        V((rows, 128), F32), V((n_kv, rows, 128), F32), V((rows, depth), BF16),
        V((n_kv, rr, cw), BF16), V((n_kv, rr, cw), BF16), V((rows, 128), F32),
        V((n_kv, rr, cw), BF16), V((rows, depth), F32), V((n_tp, rows, depth), BF16),
        V(state.shape, BF16), V(keys.shape, BF16),
        pltpu.SemaphoreType.DMA((16,)),
        dma_kv, dma_kv, dma_kv, dma_kv, dma_kv, dma_kv, dma_tp, dma_tp,
        dma_kv, dma_kv, dma_kv, dma_kv, dma_kv, dma_kv, dma_tp, dma_tp,
    ]
    specs = [ANY] * 17
    specs[11] = pl.BlockSpec(memory_space=pltpu.SMEM)
    cfg = (n_kv, n_tp, depth * n_kv, S, SP, PR, rs)
    return pl.pallas_call(
        functools.partial(kernel, cfg),
        out_shape=pltpu.VMEM((rows, depth), BF16),
        in_specs=specs,
        out_specs=pl.BlockSpec(memory_space=pltpu.VMEM),
        scratch_shapes=scratch,
        compiler_params=pltpu.CompilerParams(
            collective_id=0, has_side_effects=True, vmem_limit_bytes=60 * 1024 * 1024),
    )(*args)


def solution(mesh):
    return jax.shard_map(
        functools.partial(on_device, mesh.shape["kv"], mesh.shape["tp"]),
        mesh=mesh,
        in_specs=(
            P("grp", "kv"),
            P("kv"),
            P("kv", "tp"),
            P("kv", "tp"),
            P("kv", "tp"),
            P("kv", "tp"),
            P("kv", "tp"),
            P(("grp", "kv"), "tp", None, None),
            P(("grp", "kv"), None, "tp"),
            P(("grp", "kv"), None, "tp"),
            P(("grp", "kv"), None, "tp"),
            P(("grp", "kv")),
            P(),
            P("tp", "kv"),
            P("kv"),
            P("kv", "tp"),
            P("tp", "kv"),
        ),
        out_specs=P("grp", "kv"),
        check_vma=False,
    )
```

profile of v0, /device:TPU:0, one launch (start us, length us, event | category | flops | bytes accessed | tf_op | source)
XLA Modules:
  0.0 32.6 jit_solution(13796005180459671439)
XLA Ops:
  0.0 32.0 %shard_map.163 = bf16[12,1024]{1,0:T(8,128)(2,1)S(1)} custom-call(bf16[12,1024]{1,0:T(8,128)(2,1)} %tokens.1, bf16[1024]{0:T(1024)(128)(2,1)} %mix_gain.1, bf16[1024,512]{1,0:T(8,128)(2,1)} %wq.1, bf16[1024,512]{1,0:T(8,128)(2,1)} %wk.1, bf16[1024,512]{1,0:T(8,128)(2,1)} %wd.1, bf16[1024,1024]{1,0:T(8,128)(2,1)} %wv.1, bf16[1024,1024]{1,0:T(8,128)(2,1)} %wg.1, ...), custom_call_target="tpu_custom_call" | custom-call | tf_op jit(solution)/shard_map/pallas_call | solution.py:320
  32.0 0.6 %copy.19 = bf16[12,1024]{1,0:T(8,128)(2,1)} copy(bf16[12,1024]{1,0:T(8,128)(2,1)S(1)} %shard_map.163) | data formatting | bytes 49152
where the time goes:
time: 32.7 us; the launch traced here: 32.6 us
  Pallas kernels  32 us (98%)
  local copies, waits for them, and re-layouts  0.62 us (2%)
    pallas_call x1, Pallas kernels, on_device(): pl.pallas_call(functools.partial(kernel, cfg), out_shape=pltpu.VMEM((rows...  32 us

commit v1 on v0

v1 whole, which is shorter than its diff:
```python
import functools

import jax
import jax.numpy as jnp
from jax import lax
from jax.experimental import pallas as pl
from jax.experimental.pallas import tpu as pltpu
from jax.sharding import PartitionSpec as P

EPSILON = 1e-06
MESH = pl.DeviceIdType.MESH
F32, BF16 = jnp.float32, jnp.bfloat16
ANY = pl.BlockSpec(memory_space=pl.ANY)


def kernel(
    cfg,
    tokens, mix_gain, wq, wk, wd, wv, wg, state, keys, values, decay, lengths,
    head_gain, wo, mlp_gain, wu, wdn,
    out,
    tok_v, mix_v, wq_v, wk_v, wd_v, wv_v, wg_v, state_v, keys_v, values_v, decay_v, len_s,
    hg_v, wo_v, mg_v, wu_v, wdn_v,
    slab_a, slab_v, slab_g, recv_a, recv_v, recv_g, gath, outx, sq_own, sq_recv, mlp_lhs,
    up_send, up_recv, sq_mine, sq_all, acc, downx, mat,
    load_sem, send_sem, recv_sem, c_r,
):
    n_kv, n_tp, width, S, SP, rs, gs, halves = cfg
    rows, depth = tok_v.shape
    heads, hk, hv = state_v.shape[1:]
    positions = keys_v.shape[1]
    kcols = wq_v.shape[1]
    vcols = wv_v.shape[1]
    rr, cw = up_send.shape[1] * gs, up_send.shape[3]
    dh = depth // halves
    me = lax.axis_index("kv")
    mt = lax.axis_index("tp")

    loads = {}
    pairs = [
        (tokens, tok_v, 0), (mix_gain, mix_v, 16), (wq, wq_v, 1), (wk, wk_v, 2), (wd, wd_v, 3),
        (wv, wv_v, 4), (wg, wg_v, 5), (lengths, len_s, 6), (decay, decay_v, 7), (keys, keys_v, 8),
        (values, values_v, 9), (state, state_v, 10), (head_gain, hg_v, 11), (wo, wo_v, 12),
        (mlp_gain, mg_v, 13), (wu, wu_v, 14), (wdn, wdn_v, 15),
    ]
    for src, dst, at in pairs:
        copy = pltpu.make_async_copy(src, dst, load_sem.at[at])
        copy.start()
        loads[id(dst)] = copy

    def ready(ref):
        loads[id(ref)].wait()

    def wait_for(ref, sem):
        pltpu.make_async_copy(ref, ref, sem).wait()

    half = n_kv // 2
    low = me < half

    def kv_peer(k):
        if n_kv % 2:
            return lax.rem(me + k + 1, n_kv)
        if k < half:
            return jnp.where(low, n_kv - 1 - k, k)
        base = jnp.where(low, 0, half)
        return base + lax.rem(me - base + (k - half + 1), half)

    barrier = pltpu.get_barrier_semaphore()
    for d in range(1, n_kv):
        pl.semaphore_signal(barrier, inc=1, device_id={"kv": lax.rem(me + d, n_kv)}, device_id_type=MESH)
    for d in range(1, n_tp):
        pl.semaphore_signal(barrier, inc=1, device_id={"tp": lax.rem(mt + d, n_tp)}, device_id_type=MESH)

    sent = []

    def size_of(ref):
        size = jnp.dtype(ref.dtype).itemsize
        for n in ref.shape:
            size *= n
        return size

    def send_kv(src, dst, recv, peer, count=1):
        pltpu.make_async_remote_copy(
            src_ref=src, dst_ref=dst, send_sem=send_sem.at[0], recv_sem=recv,
            device_id={"kv": peer}, device_id_type=MESH).start()
        sent.append(count * size_of(src))

    def send_tp(src, dst, recv, d):
        pltpu.make_async_remote_copy(
            src_ref=src, dst_ref=dst, send_sem=send_sem.at[0], recv_sem=recv,
            device_id={"tp": lax.rem(mt + d, n_tp)}, device_id_type=MESH).start()
        sent.append(size_of(src))

    ready(tok_v)
    ready(mix_v)
    tok = tok_v[...].astype(F32)
    blank = [jnp.zeros((SP - S, depth), F32)] if SP > S else []
    spaced = []
    for k in range(n_kv):
        spaced += [tok[k * S:(k + 1) * S]] + blank
    if n_kv * SP % 16:
        spaced.append(jnp.zeros((16 - n_kv * SP % 16, depth), F32))
    spaced = jnp.concatenate(spaced, axis=0)
    scaled = (spaced * mix_v[...].astype(F32)[None, :]).astype(BF16)
    squares = jnp.sum(spaced * spaced, axis=1, keepdims=True)
    squares = jnp.broadcast_to(squares, (squares.shape[0], 128))
    high = squares.astype(BF16).astype(F32)
    spare = squares - high

    def spread(part, slab, at):
        for k in range(n_kv):
            slab[k, :, at:at + part.shape[1]] = part[k * SP:(k + 1) * SP].astype(BF16)

    spread(high, slab_a, 3 * kcols)
    spread(spare, slab_a, 3 * kcols + 128)
    for at, ref in enumerate((wq_v, wk_v, wd_v)):
        ready(ref)
        spread(jnp.dot(scaled, ref[...], preferred_element_type=F32), slab_a, at * kcols)
    pl.semaphore_wait(barrier, n_kv + n_tp - 2)
    for k in range(n_kv - 1):
        send_kv(slab_a.at[kv_peer(k)], recv_a.at[me], recv_sem.at[0], kv_peer(k))
    ready(wv_v)
    spread(jnp.dot(scaled, wv_v[...], preferred_element_type=F32), slab_v, 0)
    for k in range(n_kv - 1):
        send_kv(slab_v.at[kv_peer(k)], recv_v.at[me], recv_sem.at[1], kv_peer(k))
    ready(wg_v)
    spread(jnp.dot(scaled, wg_v[...], preferred_element_type=F32), slab_g, 0)
    for k in range(n_kv - 1):
        send_kv(slab_g.at[kv_peer(k)], recv_g.at[me], recv_sem.at[2], kv_peer(k))

    ready(len_s)
    ready(decay_v)
    ready(keys_v)
    ready(values_v)
    position = lax.broadcasted_iota(jnp.int32, (positions, kcols), 0)
    befores, weighted = [], []
    for b in range(S):
        length = len_s[b]
        log = decay_v[b]
        before = jnp.sum(jnp.where(position == length - 1, log, 0.0), axis=0, keepdims=True)
        befores.append(before)
        rel = jnp.where(position < length, before - log, -jnp.inf)
        weighted.append((jnp.exp(rel) * keys_v[b].astype(F32)).astype(BF16))
    befores.append(jnp.zeros((8 - S % 8, kcols), F32))
    carry = jnp.transpose(jnp.exp(jnp.concatenate(befores, axis=0)))
    ready(state_v)
    for b in range(S):
        for h in range(heads):
            inner = lax.dot_general(
                weighted[b][:, h * hk:(h + 1) * hk], values_v[b, :, h * hv:(h + 1) * hv],
                (((0,), (0,)), ((), ())), preferred_element_type=F32)
            kept = carry[h * hk:(h + 1) * hk, b:b + 1] * state_v[b, h]
            mat[h, b * hk:(b + 1) * hk, :] = (kept + inner).astype(BF16)
    ready(hg_v)

    def gathered(slab, recv):
        got = slab[me].astype(F32)
        for d in range(1, n_kv):
            got = got + recv[lax.rem(me + d, n_kv)].astype(F32)
        return got

    wait_for(recv_a.at[pl.ds(0, n_kv - 1)], recv_sem.at[0])
    got = gathered(slab_a, recv_a)
    total = got[:, 3 * kcols:3 * kcols + 1] + got[:, 3 * kcols + 128:3 * kcols + 129]
    inverse = lax.rsqrt(total / width + EPSILON)
    query = got[:, :kcols] * inverse * hk ** (-0.5)
    key = got[:, kcols:2 * kcols] * inverse
    x = got[:, 2 * kcols:3 * kcols] * inverse
    log_decay = (jnp.minimum(x, 0.0) - jnp.log1p(jnp.exp(-jnp.abs(x)))) / 16.0
    faded = query * jnp.exp(log_decay)
    product = query * key
    row = lax.broadcasted_iota(jnp.int32, (SP, hk), 0)
    heads_out, owns = [], []
    for h in range(heads):
        cols = slice(h * hk, (h + 1) * hk)
        left = jnp.concatenate(
            [jnp.where(row == b, faded[:, cols], 0.0).astype(BF16) for b in range(S)], axis=1)
        heads_out.append(jnp.dot(left, mat[h], preferred_element_type=F32))
        owns.append(jnp.sum(product[:, cols], axis=1, keepdims=True))

    wait_for(recv_v.at[pl.ds(0, n_kv - 1)], recv_sem.at[1])
    value = gathered(slab_v, recv_v) * inverse
    gain = hg_v[...].astype(F32)[None, :]
    normed = []
    for h in range(heads):
        att = heads_out[h] + owns[h] * value[:, h * hv:(h + 1) * hv]
        normed.append(att * lax.rsqrt(jnp.mean(att * att, axis=1, keepdims=True) + EPSILON) * gain)
    wait_for(recv_g.at[pl.ds(0, n_kv - 1)], recv_sem.at[2])
    gate = gathered(slab_g, recv_g) * inverse
    gate = gate * jax.nn.sigmoid(gate)
    for h in range(heads):
        cols = slice(h * hv, (h + 1) * hv)
        gath[me, :, cols] = (normed[h] * gate[:, cols]).astype(BF16)
    for k in range(n_kv - 1):
        send_kv(gath.at[me], gath.at[me], recv_sem.at[3], kv_peer(k))

    ready(wo_v)
    ready(mg_v)
    wait_for(gath.at[pl.ds(0, n_kv - 1)], recv_sem.at[3])
    merged = jnp.concatenate([gath[k].astype(F32)[:S] for k in range(n_kv)], axis=0).astype(BF16)

    def put(ref, at, part):
        for g in range(part.shape[0] // gs):
            ref[at + (g,)] = part[g * gs:(g + 1) * gs].astype(BF16)

    def get(ref, at, groups):
        return jnp.concatenate([ref[at + (g,)].astype(F32) for g in range(groups)], axis=0)

    def summed(ref, j):
        total = get(ref, (0, j), rows // gs)
        for t in range(1, n_tp):
            total = total + get(ref, (t, j), rows // gs)
        return total

    for j in range(halves):
        put(outx, (mt, j), jnp.dot(merged, wo_v[:, j * dh:(j + 1) * dh], preferred_element_type=F32))
        for d in range(1, n_tp):
            send_tp(outx.at[mt, j], outx.at[mt, j], recv_sem.at[4 + j], d)
    mixed = []
    for j in range(halves):
        wait_for(outx.at[pl.ds(0, n_tp - 1), j], recv_sem.at[4 + j])
        cols = slice(j * dh, (j + 1) * dh)
        mixed.append((tok_v[:, cols].astype(F32) + summed(outx, j)).astype(BF16).astype(F32))
        mlp_lhs[:, cols] = (mixed[j] * mg_v[cols].astype(F32)[None, :]).astype(BF16)
    ready(wu_v)

    def place(p):
        return pl.multiple_of((p // rs) * cw, 128), lax.rem(p, rs) * rr

    def up_of(p):
        col, at = place(p)
        left = mlp_lhs[...] if rs == 1 else mlp_lhs[pl.ds(pl.multiple_of(at, 16), rr), :]
        return jnp.dot(left, wu_v[:, pl.ds(col, cw)], preferred_element_type=F32)

    def up_step(peer, count=1):
        put(up_send, (peer,), up_of(peer))
        send_kv(up_send.at[peer], up_recv.at[me], recv_sem.at[7], peer, count)

    def send_squares():
        lane = lax.broadcasted_iota(jnp.int32, (rows, sq_own.shape[1]), 1)
        at = lax.broadcasted_iota(jnp.int32, (rows, sq_own.shape[1]), 0)
        squares = sum(jnp.sum(m * m, axis=1, keepdims=True) for m in mixed)
        line = jnp.sum(jnp.where(lane == at, squares, 0.0), axis=0, keepdims=True)
        sq_own[...] = jnp.broadcast_to(line, sq_own.shape)
        for k in range(n_kv - 1):
            send_kv(sq_own, sq_recv.at[me], recv_sem.at[6], kv_peer(k))

    if n_kv <= 8:
        for k in range(n_kv - 1):
            up_step(kv_peer(k))
            if k == 0:
                send_squares()
    else:
        send_squares()

        def up_loop(d, carry):
            up_step(lax.rem(me + d, n_kv), n_kv - 1)
            return carry

        lax.fori_loop(1, n_kv, up_loop, 0)
    pre = up_of(me)
    wait_for(sq_recv.at[pl.ds(0, n_kv - 1)], recv_sem.at[6])
    line = sq_own[...]
    for d in range(1, n_kv):
        line = line + sq_recv[lax.rem(me + d, n_kv)]
    lane = lax.broadcasted_iota(jnp.int32, (rows, sq_own.shape[1]), 1)
    at = lax.broadcasted_iota(jnp.int32, (rows, sq_own.shape[1]), 0)
    sq_total = jnp.sum(jnp.where(lane == at, line[:1], 0.0), axis=1, keepdims=True)
    inverse_mlp = lax.rsqrt(sq_total / width + EPSILON)
    if rs > 1:
        sq_mine[...] = jnp.broadcast_to(inverse_mlp, sq_mine.shape)
        inverse_mlp = sq_mine[pl.ds(pl.multiple_of(place(me)[1], 8), rr), :][:, :1]
    wait_for(up_recv.at[pl.ds(0, n_kv - 1)], recv_sem.at[7])
    for d in range(1, n_kv):
        pre = pre + get(up_recv, (lax.rem(me + d, n_kv),), rr // gs)
    act = jnp.maximum(pre * inverse_mlp, 0.0)
    put(sq_all, (me,), act * act)
    for k in range(n_kv - 1):
        send_kv(sq_all.at[me], sq_all.at[me], c_r.at[me], kv_peer(k))
    ready(wdn_v)

    def down_of(p, cols):
        col, at = place(p)
        left = get(sq_all, (p,), rr // gs).astype(BF16)
        return jnp.dot(left, wdn_v[pl.ds(col, cw), cols], preferred_element_type=F32), at

    def arrived(p):
        wait_for(sq_all.at[p], c_r.at[p])

    def ship(j, part):
        put(downx, (mt, j), part)
        for d in range(1, n_tp):
            send_tp(downx.at[mt, j], downx.at[mt, j], recv_sem.at[8 + j], d)

    if rs == 1 and n_kv <= 8:
        acc[...] = down_of(me, slice(None))[0]
        for k in range(n_kv - 2, 0, -1):
            arrived(kv_peer(k))
            acc[...] += down_of(kv_peer(k), slice(None))[0]
        last = kv_peer(0)
        arrived(last)
        for j in range(halves):
            cols = slice(j * dh, (j + 1) * dh)
            ship(j, acc[:, cols] + down_of(last, cols)[0])
    else:
        acc[...] = jnp.zeros_like(acc)

        def add_down(p):
            part, at = down_of(p, slice(None))
            at = pl.ds(pl.multiple_of(at, 8), rr)
            acc[at, :] = acc[at, :] + part

        add_down(me)

        def down_loop(d, carry):
            p = lax.rem(me + d, n_kv)
            arrived(p)
            add_down(p)
            return carry

        lax.fori_loop(1, n_kv, down_loop, 0)
        for j in range(halves):
            ship(j, acc[:, j * dh:(j + 1) * dh])
    for j in range(halves):
        wait_for(downx.at[pl.ds(0, n_tp - 1), j], recv_sem.at[8 + j])
        out[:, j * dh:(j + 1) * dh] = (mixed[j] + summed(downx, j)).astype(BF16)
    tiles = sum(sent) // 2048
    high, wide = wu_v.shape[0] // 8, wu_v.shape[1] // 128
    while tiles:
        fit = [m for m in range(1, wide + 1) if tiles % m == 0 and tiles // m <= high]
        m = max(fit) if fit else wide
        r = min(tiles // m, high)
        wait_for(wu_v.at[pl.ds(0, 8 * r), pl.ds(0, 128 * m)], send_sem.at[0])
        tiles -= r * m


def on_device(n_kv, n_tp, *args):
    tokens, wq, wv, state, keys, wu, wdn = (args[i] for i in (0, 2, 5, 7, 8, 15, 16))
    rows, depth = tokens.shape
    S, heads, hk, hv = state.shape
    SP = (S + 3) // 4 * 4
    kcols, vcols, hidden = wq.shape[1], wv.shape[1], wu.shape[1]
    col_splits = min(n_kv, hidden // 128)
    rs = n_kv // col_splits
    rr, cw = rows // rs, hidden // col_splits
    gs = 8 if rr % 8 == 0 else 4
    halves = 2 if depth % 256 == 0 else 1
    dh = depth // halves
    lanes = (rows + 127) // 128 * 128
    loaded = [args[i] for i in (0, 1, 2, 3, 4, 5, 6, 7, 8, 9, 10)]
    later = [args[i] for i in (12, 13, 14, 15, 16)]
    V = pltpu.VMEM
    wa = 3 * kcols + 256
    shared = V((n_tp, halves, rows // gs, gs, dh), BF16)
    hidden_part = V((n_kv, rr // gs, gs, cw), BF16)
    scratch = (
        [V(a.shape, a.dtype) for a in loaded] + [pltpu.SMEM(args[11].shape, args[11].dtype)]
        + [V(a.shape, a.dtype) for a in later] + [
            V((n_kv, SP, wa), BF16), V((n_kv, SP, vcols), BF16), V((n_kv, SP, vcols), BF16),
            V((n_kv, SP, wa), BF16), V((n_kv, SP, vcols), BF16), V((n_kv, SP, vcols), BF16),
            V((n_kv, SP, vcols), BF16), shared,
            V((4, lanes), F32), V((n_kv, 4, lanes), F32), V((rows, depth), BF16),
            hidden_part, hidden_part, V((rows, 128), F32),
            hidden_part, V((rows, depth), F32), shared,
            V((heads, S * hk, hv), BF16),
            pltpu.SemaphoreType.DMA((17,)), pltpu.SemaphoreType.DMA((1,)),
            pltpu.SemaphoreType.DMA((8 + halves,)), pltpu.SemaphoreType.DMA((n_kv,)),
        ])
    cfg = (n_kv, n_tp, depth * n_kv, S, SP, rs, gs, halves)
    return pl.pallas_call(
        functools.partial(kernel, cfg),
        out_shape=pltpu.VMEM((rows, depth), BF16),
        in_specs=[ANY] * 17,
        out_specs=pl.BlockSpec(memory_space=pltpu.VMEM),
        scratch_shapes=scratch,
        compiler_params=pltpu.CompilerParams(
            collective_id=0, has_side_effects=True, vmem_limit_bytes=60 * 1024 * 1024),
    )(*args)


def solution(mesh):
    return jax.shard_map(
        functools.partial(on_device, mesh.shape["kv"], mesh.shape["tp"]),
        mesh=mesh,
        in_specs=(
            P("grp", "kv"),
            P("kv"),
            P("kv", "tp"),
            P("kv", "tp"),
            P("kv", "tp"),
            P("kv", "tp"),
            P("kv", "tp"),
            P(("grp", "kv"), "tp", None, None),
            P(("grp", "kv"), None, "tp"),
            P(("grp", "kv"), None, "tp"),
            P(("grp", "kv"), None, "tp"),
            P(("grp", "kv")),
            P(),
            P("tp", "kv"),
            P("kv"),
            P("kv", "tp"),
            P("tp", "kv"),
        ),
        out_specs=P("grp", "kv"),
        check_vma=False,
    )
```

time: 32.7 us -> 29.8 us (0.911)
  Pallas kernels: 32 us -> 29 us
    pallas_call x1, Pallas kernels: 32 us -> 29 us  [on_device(): pl.pallas_call(functools.partial(kernel, cfg), out_shape=pltpu.VMEM((rows...]
where the time goes in v1:
time: 29.8 us; the launch traced here: 29.6 us
  Pallas kernels  29 us (97%)
  local copies, waits for them, and re-layouts  0.62 us (2%)
    pallas_call x1, Pallas kernels, on_device(): pl.pallas_call(functools.partial(kernel, cfg), out_shape=pltpu.VMEM((rows...  29 us
    unnamed x1, local copies, waits for them, and re-layouts  0.62 us

profile of v1, /device:TPU:0, one launch (start us, length us, event | category | flops | bytes accessed | tf_op | source)
XLA Modules:
  0.0 29.6 jit_solution(4809866892852805589)
XLA Ops:
  0.0 29.0 %shard_map.163 = bf16[12,1024]{1,0:T(8,128)(2,1)S(1)} custom-call(bf16[12,1024]{1,0:T(8,128)(2,1)} %tokens.1, bf16[1024]{0:T(1024)(128)(2,1)} %mix_gain.1, bf16[1024,512]{1,0:T(8,128)(2,1)} %wq.1, bf16[1024,512]{1,0:T(8,128)(2,1)} %wk.1, bf16[1024,512]{1,0:T(8,128)(2,1)} %wd.1, bf16[1024,1024]{1,0:T(8,128)(2,1)} %wv.1, bf16[1024,1024]{1,0:T(8,128)(2,1)} %wg.1, ...), custom_call_target="tpu_custom_call" | custom-call | tf_op jit(solution)/shard_map/pallas_call | solution.py:369
  29.0 0.6 %copy.19 = bf16[12,1024]{1,0:T(8,128)(2,1)} copy(bf16[12,1024]{1,0:T(8,128)(2,1)S(1)} %shard_map.163) | data formatting | bytes 49152
